TPU v7x, 32 devices: a whole 2x2x4 slice. The times are simulated.
32 devices in a mesh: grp: 2 (over y), tp: 4 (over z), dp: 4 (over x, core).
Axes of the slice: x: 2, y: 2, z: 4, core: 2. Of those that a mesh axis runs over, the one named last changes fastest.
Arguments:
- tokens: bfloat16 [64, 8, 4096], P(('grp', 'tp'), None, 'dp'), parts along dimension 0, may hold values from -6 to 6
- lengths: int32 [64], P('grp'), parts along dimension 0, may hold values from 1 to 8, 112 in all
- norm_gain: float32 [2, 4096], P(None, 'dp'), may hold values from 0.1 to 1.9
- w_recept: bfloat16 [2, 4096, 2048], P(None, 'dp', 'tp'), may hold values from -0.09375 to 0.09375
- w_key: bfloat16 [2, 4096, 2048], P(None, 'dp', 'tp'), may hold values from -0.09375 to 0.09375
- w_value: bfloat16 [2, 4096, 2048], P(None, 'dp', 'tp'), may hold values from -0.09375 to 0.09375
- w_decay: bfloat16 [2, 4096, 2048], P(None, 'dp', 'tp'), may hold values from -0.375 to 0.375
- w_rate: bfloat16 [2, 4096, 2048], P(None, 'dp', 'tp'), may hold values from -0.09375 to 0.09375
- w_gate: bfloat16 [2, 4096, 2048], P(None, 'dp', 'tp'), may hold values from -0.09375 to 0.09375
- w_out: bfloat16 [2, 2048, 4096], P(None, 'tp', 'dp'), may hold values from -0.125 to 0.125
- decay_base: float32 [2, 2048], P(None, 'tp'), may hold values from -4 to 3
- out_gain: float32 [2, 2048], P(None, 'tp'), may hold values from 0.1 to 1.9
- states: float32 [2, 64, 64, 2048], P(None, ('grp', 'dp'), None, 'tp'), parts along dimension 1, may hold values from -6 to 6
Outputs:
- stream_out: float32 [64, 8, 4096], P(('grp', 'tp'), None, 'dp'), parts along dimension 0
- new_states: float32 [2, 64, 64, 2048], P(None, ('grp', 'dp'), None, 'tp'), parts along dimension 1
There are 2 independent parts, one for each index of `grp`. A program takes and returns all parts, laid end to end along the dimension named above; an argument that names none is the same for every part. Nothing has to cross between parts.
Inputs may be any that keep to these rules, and one draw needn't show every extreme that they name: lengths[b] first tokens of sequence b are live; together they count 7 * 16 and the largest is 8.
All inputs are finite; a program needn't handle non-finite values.
Results may differ from a plain program's by a relative error of at most 0.0061.
Values may be sent and summed in bfloat16 or wider, within the bound.
A program may use at most 128 MiB of HBM per device.

v0:
```python
import jax
import jax.numpy as jnp
from jax import lax
from jax.sharding import PartitionSpec as P

D = 4096
HEAD = 64
BLOCKS = 2


group_eps = 0.00064
norm_eps = 1e-06
key_eps = 1e-06
decay_scale = 0.606531
highest = lax.Precision.HIGHEST


def mix_heads(
    state_in,
    recept,
    keys_in,
    values,
    decay_pre,
    rate_pre,
    gate_pre,
    base_shift,
    out_scale,
    live_mask,
    head_size,
):
    row_count, step_count, width_all = recept.shape
    head_count = width_all // head_size
    shape_heads = (row_count, step_count, head_count, head_size)
    decay_rate = jnp.exp(-decay_scale * jax.nn.sigmoid(decay_pre + base_shift)).reshape(shape_heads)
    learn_rate = jax.nn.sigmoid(rate_pre).reshape(shape_heads)
    key_heads = keys_in.reshape(shape_heads)
    unit_keys = key_heads * lax.rsqrt(
        jnp.sum(key_heads * key_heads, axis=3, keepdims=True) + key_eps
    )
    removal = unit_keys * learn_rate
    recept_heads = recept.reshape(shape_heads)
    value_heads = values.reshape(shape_heads)
    memory = state_in.reshape(row_count, head_size, head_count, head_size)
    outputs = []
    for position in range(step_count):
        seen_part = jnp.einsum("bihj,bhj->bhi", memory, unit_keys[:, position], precision=highest)
        updated = (
            memory * decay_rate[:, position][:, None, :, :]
            - jnp.swapaxes(seen_part, 1, 2)[:, :, :, None] * removal[:, position][:, None, :, :]
            + jnp.swapaxes(value_heads[:, position], 1, 2)[:, :, :, None]
            * key_heads[:, position][:, None, :, :]
        )
        memory = jnp.where(live_mask[:, position][:, None, None, None], updated, memory)
        outputs.append(
            jnp.einsum("bihj,bhj->bhi", memory, recept_heads[:, position], precision=highest)
        )
    readout = jnp.stack(outputs, axis=1)
    centered = readout - jnp.mean(readout, axis=3, keepdims=True)
    normed = centered * lax.rsqrt(jnp.mean(centered * centered, axis=3, keepdims=True) + group_eps)
    gated = normed.reshape(row_count, step_count, width_all) * out_scale * jax.nn.sigmoid(gate_pre)
    gated = jnp.where(live_mask[:, :, None], gated, 0.0)
    return (gated.astype(jnp.bfloat16), memory.reshape(row_count, head_size, width_all))


def body(
    tokens,
    lengths,
    norm_gain,
    w_recept,
    w_key,
    w_value,
    w_decay,
    w_rate,
    w_gate,
    w_out,
    decay_base,
    out_gain,
    states,
):
    horizon = tokens.shape[1]
    held_rows = states.shape[1]
    first_row = lax.axis_index("dp") * held_rows
    held_lengths = lax.dynamic_slice_in_dim(lengths, first_row, held_rows, 0)
    live_mask = jnp.arange(horizon, dtype=jnp.int32)[None, :] < held_lengths[:, None]
    current = tokens.astype(jnp.float32)
    finals = []
    for block_index in range(BLOCKS):
        gathered_in = lax.all_gather(current, "tp", axis=0, tiled=True)
        squares = jnp.sum(jnp.square(gathered_in), axis=2)
        total_squares = lax.psum_scatter(squares, "dp", scatter_dimension=0, tiled=True)
        inv_rms = lax.rsqrt(total_squares / D + norm_eps)
        scaled = (gathered_in * norm_gain[block_index]).astype(jnp.bfloat16)
        partials = tuple(
            (
                jnp.einsum(
                    "bsd,dc->bsc", scaled, weight[block_index], preferred_element_type=jnp.float32
                )
                for weight in (w_recept, w_key, w_value, w_decay, w_rate, w_gate)
            )
        )
        summed = lax.psum_scatter(partials, "dp", scatter_dimension=0, tiled=True)
        projected = [member * inv_rms[:, :, None] for member in summed]
        gated, final_state = mix_heads(
            states[block_index],
            projected[0],
            projected[1],
            projected[2],
            projected[3],
            projected[4],
            projected[5],
            decay_base[block_index],
            out_gain[block_index],
            live_mask,
            HEAD,
        )
        finals.append(final_state)
        all_rows = lax.all_gather(gated, "dp", axis=0, tiled=True)
        regrouped = lax.all_to_all(all_rows, "tp", split_axis=0, concat_axis=2, tiled=True)
        output = jnp.einsum(
            "bsc,cd->bsd",
            regrouped,
            lax.all_gather(w_out[block_index], "tp", axis=0, tiled=True),
            preferred_element_type=jnp.float32,
        )
        current = current + output
    return (current, jnp.stack(finals, axis=0))


def solution(mesh):
    in_specs = (
        P(("grp", "tp"), None, "dp"),
        P("grp"),
        P(None, "dp"),
        P(None, "dp", "tp"),
        P(None, "dp", "tp"),
        P(None, "dp", "tp"),
        P(None, "dp", "tp"),
        P(None, "dp", "tp"),
        P(None, "dp", "tp"),
        P(None, "tp", "dp"),
        P(None, "tp"),
        P(None, "tp"),
        P(None, ("grp", "dp"), None, "tp"),
    )
    out_specs = (P(("grp", "tp"), None, "dp"), P(None, ("grp", "dp"), None, "tp"))
    return jax.shard_map(body, mesh=mesh, in_specs=in_specs, out_specs=out_specs, check_vma=False)
```

profile of v0, /device:TPU:0, one launch (start us, length us, event | category | flops | bytes accessed | tf_op | source)
XLA Modules:
  0.0 758.3 jit_solution(8555726532389750007)
XLA Ops:
  10.4 30.4 %all-gather.7.cloned.1.call-done = f32[32,8,1024]{2,1,0:T(8,128)} async-done(((f32[8,8,1024]{2,1,0:T(8,128)}), f32[32,8,1024]{2,1,0:T(8,128)}) %all-gather.7.cloned.1.call-update) | async-done | bytes 1048592 | tf_op jit(solution)/shard_map/all_gather | solution.py:88
  54.3 3.2 fusion.112
  64.6 10.8 %all-reduce = f32[32,8]{1,0:T(8,128)S(1)} all-reduce(f32[32,8]{1,0:T(8,128)S(1)} %get-tuple-element.12), channel_id=5, replica_groups=mesh['grp'=2,'tp'=4,'dp'=4] {'dp'}, use_global_device_ids=true, to_apply=%region_2.0.clone | all-reduce | flops 256 | bytes 2048
  75.4 13.5 %reduce-scatter.15.cloned.1.call-done = f32[8,8,512]{2,1,0:T(8,128)} async-done(((f32[32,8,512]{2,1,0:T(8,128)}), f32[8,8,512]{2,1,0:T(8,128)}) %reduce-scatter.15.cloned.1.call-update) | async-done | bytes 131088 | tf_op jit(solution)/shard_map/reduce_scatter | solution.py:101
  88.9 24.0 %reduce-scatter.17.cloned.1.call-done = f32[8,8,512]{2,1,0:T(8,128)} async-done(((f32[32,8,512]{2,1,0:T(8,128)}), f32[8,8,512]{2,1,0:T(8,128)}) %reduce-scatter.17.cloned.1.call-update) | async-done | bytes 131088 | tf_op jit(solution)/shard_map/reduce_scatter | solution.py:101
  113.0 24.0 %reduce-scatter.19.cloned.1.call-done = f32[8,8,512]{2,1,0:T(8,128)} async-done(((f32[32,8,512]{2,1,0:T(8,128)}), f32[8,8,512]{2,1,0:T(8,128)}) %reduce-scatter.19.cloned.1.call-update) | async-done | bytes 131088 | tf_op jit(solution)/shard_map/reduce_scatter | solution.py:101
  137.0 24.0 %reduce-scatter.21.cloned.1.call-done = f32[8,8,512]{2,1,0:T(8,128)} async-done(((f32[32,8,512]{2,1,0:T(8,128)}), f32[8,8,512]{2,1,0:T(8,128)}) %reduce-scatter.21.cloned.1.call-update) | async-done | bytes 131088 | tf_op jit(solution)/shard_map/reduce_scatter | solution.py:101
  173.7 3.4 fusion.60
  178.2 3.3 add_select_fusion.14
  183.0 4.1 fusion.56
  190.3 5.1 add_select_fusion.13
  196.7 4.1 fusion.52
  204.0 5.8 add_select_fusion.12
  211.2 4.1 fusion.48
  218.4 7.1 add_select_fusion.11
  226.8 4.1 fusion.44
  234.1 8.6 %add_select_fusion.10 = f32[8,64,8,64]{3,2,1,0:T(8,128)S(1)} fusion(f32[8,8,64]{2,1,0:T(8,128)} %get-tuple-element.52, f32[8,64,8]{2,1,0:T(8,128)} %copy.40, f32[8,8,64]{2,1,0:T(8,128)} %get-tuple-element.36, f32[8,64,8]{2,1,0:T(8,128)} %bitcast.789, f32[8,8,64]{2,1,0:T(8,128)} %get-tuple-element.20, pred[8]{0:T(512)(128)(4,1)} %get-tuple-element.176, ...), kind=kLoop, calls=%fused_computation.21 | loop fusion | flops 9437184 | bytes 2588720 | tf_op jit(solution)/shard_map/jit(_where)/select_n | solution.py:53
  244.0 4.1 fusion.40
  251.2 10.0 %add_select_fusion.9 = f32[8,64,8,64]{3,2,1,0:T(8,128)S(1)} fusion(f32[8,8,64]{2,1,0:T(8,128)} %get-tuple-element.53, f32[8,64,8]{2,1,0:T(8,128)} %copy.41, f32[8,8,64]{2,1,0:T(8,128)} %get-tuple-element.37, f32[8,64,8]{2,1,0:T(8,128)} %bitcast.797, f32[8,8,64]{2,1,0:T(8,128)} %get-tuple-element.21, pred[8]{0:T(512)(128)(4,1)} %get-tuple-element.175, ...), kind=kLoop, calls=%fused_computation.20 | loop fusion | flops 11010048 | bytes 2670648 | tf_op jit(solution)/shard_map/jit(_where)/select_n | solution.py:53
  262.6 4.1 fusion.36
  268.2 5.2 fusion.62
  274.0 4.4 fusion.58
  279.1 4.4 fusion.54
  284.1 4.8 fusion.50
  289.5 4.4 fusion.46
  294.7 4.4 fusion.42
  299.7 4.2 fusion.38
  304.7 10.8 %add_select_fusion.8 = f32[8,64,8,64]{3,2,1,0:T(8,128)S(1)} fusion(f32[8,8,64]{2,1,0:T(8,128)} %get-tuple-element.54, f32[8,64,8]{2,1,0:T(8,128)S(1)} %copy-done.51, f32[8,8,64]{2,1,0:T(8,128)} %get-tuple-element.38, f32[8,64,8]{2,1,0:T(8,128)S(1)} %bitcast.804, f32[8,8,64]{2,1,0:T(8,128)} %get-tuple-element.22, pred[8]{0:T(512)(128)(4,1)S(1)} %copy-done.161, ...), kind=kLoop, calls=%fused_computation.19 | loop fusion | flops 12582912 | bytes 2752576 | tf_op jit(solution)/shard_map/jit(_where)/select_n | solution.py:53
  315.7 3.5 fusion.6
  324.7 5.8 all_gather.19
  330.4 13.7 %all_to_all.36 = bf16[32,8,512]{2,1,0:T(8,128)(2,1)S(1)} all-to-all(bf16[32,8,512]{2,1,0:T(8,128)(2,1)S(1)} %all_gather.19), channel_id=1, replica_groups=mesh['grp'=2,'tp'=4,'dp'=4] {'tp'}, dimensions={0} | all-to-all | bytes 524288 | tf_op jit(solution)/shard_map/all_to_all | solution.py:118
  344.3 3.7 fusion.64
  348.1 26.2 %all-gather.9.cloned.1.call-done = f32[32,8,1024]{2,1,0:T(8,128)} async-done(((f32[8,8,1024]{2,1,0:T(8,128)}), f32[32,8,1024]{2,1,0:T(8,128)}) %all-gather.9.cloned.1.call-update) | async-done | bytes 1048592 | tf_op jit(solution)/shard_map/all_gather | solution.py:88
  410.7 2.9 mul.1503
  433.1 2.9 mul.1481
  451.8 3.1 mul.1671
  492.1 8.9 %add_select_fusion.17 = f32[1,8,64,512]{3,2,1,0:T(8,128)} fusion(f32[1,8,64,512]{3,2,1,0:T(8,128)S(1)} %copy-done.48, f32[1,8,64,512]{3,2,1,0:T(8,128)} %mul.1722, f32[1,8,64,512]{3,2,1,0:T(8,128)} %mul.1715, f32[1,8,64,512]{3,2,1,0:T(8,128)} %mul.1711, f32[1,8,64,512]{3,2,1,0:T(8,128)} %mul.1704, f32[1,8,64,512]{3,2,1,0:T(8,128)} %mul.1700, ...), kind=kLoop, calls=%fused_computation.110 | loop fusion | flops 12582912 | bytes 19267648 | tf_op jit(solution)/shard_map/jit(_where)/select_n | solution.py:53
  501.0 10.7 %all-reduce.1 = f32[32,8]{1,0:T(8,128)S(1)} all-reduce(f32[32,8]{1,0:T(8,128)S(1)} %copy-done.146), channel_id=12, replica_groups=mesh['grp'=2,'tp'=4,'dp'=4] {'dp'}, use_global_device_ids=true, to_apply=%region_13.14.clone | all-reduce | flops 256 | bytes 2048
  522.4 3.5 fusion.34
  526.6 5.0 fusion.32
  532.7 3.6 add_select_fusion.6
  536.3 4.1 fusion.30
  540.4 4.1 fusion.28
  547.6 4.6 add_select_fusion.5
  553.5 4.1 fusion.24
  560.8 6.2 add_select_fusion.4
  568.4 4.1 fusion.20
  575.7 7.1 add_select_fusion.3
  584.1 4.1 fusion.16
  591.4 8.4 %add_select_fusion.2 = f32[8,64,8,64]{3,2,1,0:T(8,128)S(1)} fusion(f32[8,8,64]{2,1,0:T(8,128)} %get-tuple-element.100, f32[8,64,8]{2,1,0:T(8,128)} %copy.49, f32[8,8,64]{2,1,0:T(8,128)} %get-tuple-element.84, f32[8,64,8]{2,1,0:T(8,128)} %bitcast.793, f32[8,8,64]{2,1,0:T(8,128)} %get-tuple-element.68, pred[8]{0:T(512)(128)(4,1)} %get-tuple-element.176, ...), kind=kLoop, calls=%fused_computation.13 | loop fusion | flops 9437184 | bytes 2588720 | tf_op jit(solution)/shard_map/jit(_where)/select_n | solution.py:53
  601.2 4.1 fusion.12
  606.9 9.9 %add_select_fusion.1 = f32[8,64,8,64]{3,2,1,0:T(8,128)S(1)} fusion(f32[8,8,64]{2,1,0:T(8,128)} %get-tuple-element.101, f32[8,64,8]{2,1,0:T(8,128)} %copy.50, f32[8,8,64]{2,1,0:T(8,128)} %get-tuple-element.85, f32[8,64,8]{2,1,0:T(8,128)} %bitcast.800, f32[8,8,64]{2,1,0:T(8,128)} %get-tuple-element.69, pred[8]{0:T(512)(128)(4,1)} %get-tuple-element.175, ...), kind=kLoop, calls=%fused_computation.12 | loop fusion | flops 11010048 | bytes 2670648 | tf_op jit(solution)/shard_map/jit(_where)/select_n | solution.py:53
  618.1 4.1 fusion.8
  626.0 5.2 fusion.26
  631.8 4.4 fusion.22
  636.8 4.4 fusion.18
  642.0 4.6 fusion.14
  647.2 4.2 fusion.10
  652.3 10.7 %add_select_fusion = f32[8,64,8,64]{3,2,1,0:T(8,128)S(1)} fusion(f32[8,8,64]{2,1,0:T(8,128)} %get-tuple-element.102, f32[8,64,8]{2,1,0:T(8,128)} %copy.51, f32[8,8,64]{2,1,0:T(8,128)} %get-tuple-element.86, f32[8,64,8]{2,1,0:T(8,128)S(1)} %bitcast.806, f32[8,8,64]{2,1,0:T(8,128)} %get-tuple-element.70, pred[8]{0:T(512)(128)(4,1)S(1)} %copy-done.162, ...), kind=kLoop, calls=%fused_computation.11 | loop fusion | flops 12582912 | bytes 2752576 | tf_op jit(solution)/shard_map/jit(_where)/select_n | solution.py:53
  663.1 3.5 fusion.4
  672.1 6.2 all_gather.22
  678.3 4.4 all-to-all-start.1
  737.0 8.3 %add_select_fusion.16 = f32[1,8,64,512]{3,2,1,0:T(8,128)S(1)} fusion(f32[1,8,64,512]{3,2,1,0:T(8,128)} %mul.1814, f32[1,8,64,512]{3,2,1,0:T(8,128)} %mul.1810, f32[1,8,64,512]{3,2,1,0:T(8,128)} %mul.1803, f32[1,8,64,512]{3,2,1,0:T(8,128)} %mul.1799, f32[1,8,64,512]{3,2,1,0:T(8,128)} %mul.1792, f32[1,8,64,512]{3,2,1,0:T(8,128)} %mul.1788, ...), kind=kLoop, calls=%fused_computation.109 | loop fusion | flops 12582912 | bytes 19267648 | tf_op jit(solution)/shard_map/jit(_where)/select_n | solution.py:53
  747.9 3.7 fusion.67
  (651 shorter events, 283.4 us)
Async XLA Ops:
  7.2 35.1 %copy-start.171 = (bf16[2,1024,512]{2,1,0:T(8,128)(2,1)S(1)}, bf16[2,1024,512]{2,1,0:T(8,128)(2,1)}, u32[]{:S(2)}) copy-start(bf16[2,1024,512]{2,1,0:T(8,128)(2,1)} %param.19) | copy-start | bytes 6291460
  7.2 33.7 %all-gather.7.cloned.1.call-start = ((), (), s32[]{:S(2)}) async-start(), calls=%async_computation.14 | async-start | bytes 1310720 | tf_op jit(solution)/shard_map/all_gather | solution.py:88
  9.0 66.4 %reduce-scatter.13.cloned.1.call-start = ((), (), s32[]{:S(2)}) async-start(), calls=%async_computation.15 | async-start | bytes 655360 | tf_op jit(solution)/shard_map/reduce_scatter | solution.py:101
  43.6 45.4 %reduce-scatter.15.cloned.1.call-start = ((), (), s32[]{:S(2)}) async-start(), calls=%async_computation.16 | async-start | bytes 655360 | tf_op jit(solution)/shard_map/reduce_scatter | solution.py:101
  46.2 66.7 %reduce-scatter.17.cloned.1.call-start = ((), (), s32[]{:S(2)}) async-start(), calls=%async_computation.17 | async-start | bytes 655360 | tf_op jit(solution)/shard_map/reduce_scatter | solution.py:101
  47.6 89.4 %reduce-scatter.19.cloned.1.call-start = ((), (), s32[]{:S(2)}) async-start(), calls=%async_computation.18 | async-start | bytes 655360 | tf_op jit(solution)/shard_map/reduce_scatter | solution.py:101
  50.4 110.7 %reduce-scatter.21.cloned.1.call-start = ((), (), s32[]{:S(2)}) async-start(), calls=%async_computation.19 | async-start | bytes 655360 | tf_op jit(solution)/shard_map/reduce_scatter | solution.py:101
  51.7 271.9 %reduce-scatter.23.cloned.1.call-start = ((), (), s32[]{:S(2)}) async-start(), calls=%async_computation.20 | async-start | bytes 655360 | tf_op jit(solution)/shard_map/reduce_scatter | solution.py:101
  54.3 290.0 %all-gather.11.cloned.1.call-start = ((), (), s32[]{:S(2)}) async-start(), calls=%async_computation.28 | async-start | bytes 5242880 | tf_op jit(solution)/shard_map/all_gather | solution.py:122
  57.5 316.8 %all-gather.9.cloned.1.call-start = ((), (), s32[]{:S(2)}) async-start(), calls=%async_computation.21 | async-start | bytes 1310720 | tf_op jit(solution)/shard_map/all_gather | solution.py:88
  75.4 87.7 %copy-start.155 = (f32[8,8]{1,0:T(8,128)}, f32[8,8]{1,0:T(8,128)S(1)}, u32[]{:S(2)}) copy-start(f32[8,8]{1,0:T(8,128)S(1)} %fusion.109) | copy-start | bytes 772
  251.2 11.3 %copy-start.98 = (f32[8,1,8,64]{3,2,1,0:T(8,128)S(1)}, f32[8,1,8,64]{3,2,1,0:T(8,128)}, u32[]{:S(2)}) copy-start(f32[8,1,8,64]{3,2,1,0:T(8,128)} %get-tuple-element.134) | copy-start | bytes 49156
  268.2 10.8 %copy-start.13 = (f32[8,64,8,64]{3,2,1,0:T(8,128)S(1)}, f32[8,64,8,64]{3,2,1,0:T(8,128)}, u32[]{:S(2)}) copy-start(f32[8,64,8,64]{3,2,1,0:T(8,128)} %copy-done.12) | copy-start | bytes 3145732
  278.4 10.4 %copy-start.71 = (f32[8,8,1,64]{3,2,1,0:T(1,128)}, f32[8,8,1,64]{3,2,1,0:T(1,128)S(1)}, u32[]{:S(2)}) copy-start(f32[8,8,1,64]{3,2,1,0:T(1,128)S(1)} %fusion.58) | copy-start | bytes 49156
  279.0 10.4 %copy-start.20 = (f32[8,64,8,64]{3,2,1,0:T(8,128)S(1)}, f32[8,64,8,64]{3,2,1,0:T(8,128)}, u32[]{:S(2)}) copy-start(f32[8,64,8,64]{3,2,1,0:T(8,128)} %copy-done.19) | copy-start | bytes 3145732
  283.4 10.4 %copy-start.73 = (f32[8,8,1,64]{3,2,1,0:T(1,128)}, f32[8,8,1,64]{3,2,1,0:T(1,128)S(1)}, u32[]{:S(2)}) copy-start(f32[8,8,1,64]{3,2,1,0:T(1,128)S(1)} %fusion.54) | copy-start | bytes 49156
  284.1 10.4 %copy-start.2 = (f32[8,64,8,64]{3,2,1,0:T(8,128)S(1)}, f32[8,64,8,64]{3,2,1,0:T(8,128)}, u32[]{:S(2)}) copy-start(f32[8,64,8,64]{3,2,1,0:T(8,128)} %copy-done.1) | copy-start | bytes 3145732
  289.5 10.2 %copy-start.4 = (f32[8,64,8,64]{3,2,1,0:T(8,128)S(1)}, f32[8,64,8,64]{3,2,1,0:T(8,128)}, u32[]{:S(2)}) copy-start(f32[8,64,8,64]{3,2,1,0:T(8,128)} %copy-done.3) | copy-start | bytes 3145732
  299.0 16.5 %copy-start.85 = (f32[8,8,1,64]{3,2,1,0:T(1,128)}, f32[8,8,1,64]{3,2,1,0:T(1,128)S(1)}, u32[]{:S(2)}) copy-start(f32[8,8,1,64]{3,2,1,0:T(1,128)S(1)} %fusion.42) | copy-start | bytes 49156
  304.7 10.9 %copy-start.93 = (f32[8,1,8,64]{3,2,1,0:T(8,128)S(1)}, f32[8,1,8,64]{3,2,1,0:T(8,128)}, u32[]{:S(2)}) copy-start(f32[8,1,8,64]{3,2,1,0:T(8,128)} %get-tuple-element.150) | copy-start | bytes 49156
  322.1 22.2 %copy-start.64 = (bf16[8,8,1024]{2,1,0:T(8,128)(2,1)S(1)}, bf16[8,8,1024]{2,1,0:T(8,128)(2,1)}, u32[]{:S(2)}) copy-start(bf16[8,8,1024]{2,1,0:T(8,128)(2,1)} %param.13) | copy-start | bytes 393220
  344.3 30.0 %copy-start.160 = (f32[1,1024]{1,0:T(1,128)S(1)}, f32[1,1024]{1,0:T(1,128)}, u32[]{:S(2)}) copy-start(f32[1,1024]{1,0:T(1,128)} %get-tuple-element.158) | copy-start | bytes 12292
  348.0 163.7 %reduce-scatter.25.cloned.1.call-start = ((), (), s32[]{:S(2)}) async-start(), calls=%async_computation.22 | async-start | bytes 655360 | tf_op jit(solution)/shard_map/reduce_scatter | solution.py:101
  378.8 132.9 %reduce-scatter.27.cloned.1.call-start = ((), (), s32[]{:S(2)}) async-start(), calls=%async_computation.23 | async-start | bytes 655360 | tf_op jit(solution)/shard_map/reduce_scatter | solution.py:101
  381.4 130.4 %reduce-scatter.29.cloned.1.call-start = ((), (), s32[]{:S(2)}) async-start(), calls=%async_computation.24 | async-start | bytes 655360 | tf_op jit(solution)/shard_map/reduce_scatter | solution.py:101
  383.9 127.9 %reduce-scatter.31.cloned.1.call-start = ((), (), s32[]{:S(2)}) async-start(), calls=%async_computation.25 | async-start | bytes 655360 | tf_op jit(solution)/shard_map/reduce_scatter | solution.py:101
  386.5 125.4 %reduce-scatter.33.cloned.1.call-start = ((), (), s32[]{:S(2)}) async-start(), calls=%async_computation.26 | async-start | bytes 655360 | tf_op jit(solution)/shard_map/reduce_scatter | solution.py:101
  389.0 282.0 %reduce-scatter.35.cloned.1.call-start = ((), (), s32[]{:S(2)}) async-start(), calls=%async_computation.27 | async-start | bytes 655360 | tf_op jit(solution)/shard_map/reduce_scatter | solution.py:101
  391.6 356.2 %all-gather.13.cloned.1.call-start = ((), (), s32[]{:S(2)}) async-start(), calls=%async_computation.29 | async-start | bytes 5242880 | tf_op jit(solution)/shard_map/all_gather | solution.py:122
  475.4 12.2 %copy-start.113 = (f32[8,1,8,64]{3,2,1,0:T(8,128)S(1)}, f32[8,1,8,64]{3,2,1,0:T(8,128)}, u32[]{:S(2)}) copy-start(f32[8,1,8,64]{3,2,1,0:T(8,128)} %get-tuple-element.59) | copy-start | bytes 49156
  475.4 12.9 %copy-start.121 = (f32[8,1,8,64]{3,2,1,0:T(8,128)S(1)}, f32[8,1,8,64]{3,2,1,0:T(8,128)}, u32[]{:S(2)}) copy-start(f32[8,1,8,64]{3,2,1,0:T(8,128)} %get-tuple-element.43) | copy-start | bytes 49156
  475.4 13.8 %copy-start.112 = (f32[8,1,8,64]{3,2,1,0:T(8,128)S(1)}, f32[8,1,8,64]{3,2,1,0:T(8,128)}, u32[]{:S(2)}) copy-start(f32[8,1,8,64]{3,2,1,0:T(8,128)} %get-tuple-element.60) | copy-start | bytes 49156
  475.4 13.9 %copy-start.120 = (f32[8,1,8,64]{3,2,1,0:T(8,128)S(1)}, f32[8,1,8,64]{3,2,1,0:T(8,128)}, u32[]{:S(2)}) copy-start(f32[8,1,8,64]{3,2,1,0:T(8,128)} %get-tuple-element.44) | copy-start | bytes 49156
  475.4 14.8 %copy-start.111 = (f32[8,1,8,64]{3,2,1,0:T(8,128)S(1)}, f32[8,1,8,64]{3,2,1,0:T(8,128)}, u32[]{:S(2)}) copy-start(f32[8,1,8,64]{3,2,1,0:T(8,128)} %get-tuple-element.61) | copy-start | bytes 49156
  475.4 14.8 %copy-start.119 = (f32[8,1,8,64]{3,2,1,0:T(8,128)S(1)}, f32[8,1,8,64]{3,2,1,0:T(8,128)}, u32[]{:S(2)}) copy-start(f32[8,1,8,64]{3,2,1,0:T(8,128)} %get-tuple-element.45) | copy-start | bytes 49156
  475.4 15.7 %copy-start.110 = (f32[8,1,8,64]{3,2,1,0:T(8,128)S(1)}, f32[8,1,8,64]{3,2,1,0:T(8,128)}, u32[]{:S(2)}) copy-start(f32[8,1,8,64]{3,2,1,0:T(8,128)} %get-tuple-element.46) | copy-start | bytes 49156
  475.4 15.8 %copy-start.118 = (f32[8,1,8,64]{3,2,1,0:T(8,128)S(1)}, f32[8,1,8,64]{3,2,1,0:T(8,128)}, u32[]{:S(2)}) copy-start(f32[8,1,8,64]{3,2,1,0:T(8,128)} %get-tuple-element.30) | copy-start | bytes 49156
  475.4 16.7 %copy-start.48 = (f32[1,8,64,512]{3,2,1,0:T(8,128)S(1)}, f32[1,8,64,512]{3,2,1,0:T(8,128)}, u32[]{:S(2)}) copy-start(f32[1,8,64,512]{3,2,1,0:T(8,128)} %mul.1726) | copy-start | bytes 3145732
  492.1 19.7 %copy-start.167 = (f32[1,512]{1,0:T(1,128)S(1)}, f32[1,512]{1,0:T(1,128)}, u32[]{:S(2)}) copy-start(f32[1,512]{1,0:T(1,128)} %get-tuple-element.167) | copy-start | bytes 6148
  606.9 11.2 %copy-start.97 = (f32[8,1,8,64]{3,2,1,0:T(8,128)S(1)}, f32[8,1,8,64]{3,2,1,0:T(8,128)}, u32[]{:S(2)}) copy-start(f32[8,1,8,64]{3,2,1,0:T(8,128)} %get-tuple-element.110) | copy-start | bytes 49156
  626.0 10.8 %copy-start.22 = (f32[8,64,8,64]{3,2,1,0:T(8,128)S(1)}, f32[8,64,8,64]{3,2,1,0:T(8,128)}, u32[]{:S(2)}) copy-start(f32[8,64,8,64]{3,2,1,0:T(8,128)} %copy-done.21) | copy-start | bytes 3145732
  636.8 10.4 %copy-start.8 = (f32[8,64,8,64]{3,2,1,0:T(8,128)S(1)}, f32[8,64,8,64]{3,2,1,0:T(8,128)}, u32[]{:S(2)}) copy-start(f32[8,64,8,64]{3,2,1,0:T(8,128)} %copy-done.7) | copy-start | bytes 3145732
  641.8 10.3 %copy-start.25 = (f32[8,8,1,64]{1,3,0,2:T(8,128)S(1)}, f32[8,8,1,64]{1,3,0,2:T(8,128)}, u32[]{:S(2)}) copy-start(f32[8,8,1,64]{1,3,0,2:T(8,128)} %copy.112) | copy-start | bytes 49156
  641.8 10.3 %copy-start.29 = (f32[8,64,8]{2,1,0:T(8,128)S(1)}, f32[8,64,8]{2,1,0:T(8,128)}, u32[]{:S(2)}) copy-start(f32[8,64,8]{2,1,0:T(8,128)} %copy.47) | copy-start | bytes 49156
  641.8 10.3 %copy-start.31 = (f32[8,8,1,64]{1,3,0,2:T(8,128)S(1)}, f32[8,8,1,64]{1,3,0,2:T(8,128)}, u32[]{:S(2)}) copy-start(f32[8,8,1,64]{1,3,0,2:T(8,128)} %copy.117) | copy-start | bytes 49156
  641.9 10.2 %copy-start.35 = (f32[8,64,8]{2,1,0:T(8,128)S(1)}, f32[8,64,8]{2,1,0:T(8,128)}, u32[]{:S(2)}) copy-start(f32[8,64,8]{2,1,0:T(8,128)} %copy.48) | copy-start | bytes 49156
  641.9 10.2 %copy-start.37 = (f32[8,8,1,64]{1,3,0,2:T(8,128)S(1)}, f32[8,8,1,64]{1,3,0,2:T(8,128)}, u32[]{:S(2)}) copy-start(f32[8,8,1,64]{1,3,0,2:T(8,128)} %copy.122) | copy-start | bytes 49156
  641.9 10.2 %copy-start.42 = (f32[8,64,8]{2,1,0:T(8,128)S(1)}, f32[8,64,8]{2,1,0:T(8,128)}, u32[]{:S(2)}) copy-start(f32[8,64,8]{2,1,0:T(8,128)} %copy.49) | copy-start | bytes 49156
  641.9 10.2 %copy-start.43 = (f32[8,8,1,64]{1,3,0,2:T(8,128)S(1)}, f32[8,8,1,64]{1,3,0,2:T(8,128)}, u32[]{:S(2)}) copy-start(f32[8,8,1,64]{1,3,0,2:T(8,128)} %copy.127) | copy-start | bytes 49156
  641.9 10.2 %copy-start.46 = (f32[8,64,8]{2,1,0:T(8,128)S(1)}, f32[8,64,8]{2,1,0:T(8,128)}, u32[]{:S(2)}) copy-start(f32[8,64,8]{2,1,0:T(8,128)} %copy.50) | copy-start | bytes 49156
  641.9 10.2 %copy-start.47 = (f32[8,8,1,64]{1,3,0,2:T(8,128)S(1)}, f32[8,8,1,64]{1,3,0,2:T(8,128)}, u32[]{:S(2)}) copy-start(f32[8,8,1,64]{1,3,0,2:T(8,128)} %copy.132) | copy-start | bytes 49156
  641.9 10.2 %copy-start.53 = (f32[8,8,1,64]{1,3,0,2:T(8,128)S(1)}, f32[8,8,1,64]{1,3,0,2:T(8,128)}, u32[]{:S(2)}) copy-start(f32[8,8,1,64]{1,3,0,2:T(8,128)} %copy.137) | copy-start | bytes 49156
  641.9 10.2 %copy-start.55 = (f32[8,8,64]{2,1,0:T(8,128)S(1)}, f32[8,8,64]{2,1,0:T(8,128)}, u32[]{:S(2)}) copy-start(f32[8,8,64]{2,1,0:T(8,128)} %get-tuple-element.80) | copy-start | bytes 49156
  641.9 10.2 %copy-start.57 = (f32[8,8,64]{2,1,0:T(8,128)S(1)}, f32[8,8,64]{2,1,0:T(8,128)}, u32[]{:S(2)}) copy-start(f32[8,8,64]{2,1,0:T(8,128)} %get-tuple-element.64) | copy-start | bytes 49156
  641.9 10.2 %copy-start.59 = (f32[8,8,64]{2,1,0:T(8,128)S(1)}, f32[8,8,64]{2,1,0:T(8,128)}, u32[]{:S(2)}) copy-start(f32[8,8,64]{2,1,0:T(8,128)} %get-tuple-element.97) | copy-start | bytes 49156
  642.0 10.2 %copy-start.61 = (f32[8,8,64]{2,1,0:T(8,128)S(1)}, f32[8,8,64]{2,1,0:T(8,128)}, u32[]{:S(2)}) copy-start(f32[8,8,64]{2,1,0:T(8,128)} %get-tuple-element.81) | copy-start | bytes 49156
  642.0 10.2 %copy-start.63 = (f32[8,8,64]{2,1,0:T(8,128)S(1)}, f32[8,8,64]{2,1,0:T(8,128)}, u32[]{:S(2)}) copy-start(f32[8,8,64]{2,1,0:T(8,128)} %get-tuple-element.65) | copy-start | bytes 49156
  642.0 10.2 %copy-start.148 = (pred[8]{0:T(512)(128)(4,1)S(1)}, pred[8]{0:T(512)(128)(4,1)}, u32[]{:S(2)}) copy-start(pred[8]{0:T(512)(128)(4,1)} %get-tuple-element.177) | copy-start | bytes 28
  642.0 10.2 %copy-start.151 = (pred[8]{0:T(512)(128)(4,1)S(1)}, pred[8]{0:T(512)(128)(4,1)}, u32[]{:S(2)}) copy-start(pred[8]{0:T(512)(128)(4,1)} %get-tuple-element.176) | copy-start | bytes 28
  642.0 10.2 %copy-start.158 = (pred[8]{0:T(512)(128)(4,1)S(1)}, pred[8]{0:T(512)(128)(4,1)}, u32[]{:S(2)}) copy-start(pred[8]{0:T(512)(128)(4,1)} %get-tuple-element.175) | copy-start | bytes 28
  642.0 10.2 %copy-start.162 = (pred[8]{0:T(512)(128)(4,1)S(1)}, pred[8]{0:T(512)(128)(4,1)}, u32[]{:S(2)}) copy-start(pred[8]{0:T(512)(128)(4,1)} %get-tuple-element.174) | copy-start | bytes 28
  646.6 16.4 %copy-start.87 = (f32[8,8,1,64]{3,2,1,0:T(1,128)}, f32[8,8,1,64]{3,2,1,0:T(1,128)S(1)}, u32[]{:S(2)}) copy-start(f32[8,8,1,64]{3,2,1,0:T(1,128)S(1)} %fusion.14) | copy-start | bytes 49156
  652.3 10.8 %copy-start.94 = (f32[8,1,8,64]{3,2,1,0:T(8,128)S(1)}, f32[8,1,8,64]{3,2,1,0:T(8,128)}, u32[]{:S(2)}) copy-start(f32[8,1,8,64]{3,2,1,0:T(8,128)} %get-tuple-element.126) | copy-start | bytes 49156
  678.3 68.5 %all-to-all-start.1 = ((bf16[32,8,512]{2,1,0:T(8,128)(2,1)}), bf16[32,8,512]{2,1,0:T(8,128)(2,1)}, u32[]{:S(2)}, u32[]{:S(2)}) async-start(bf16[32,8,512]{2,1,0:T(8,128)(2,1)} %all_gather.22), calls=%async_computation.13 | async-start | bytes 524288 | tf_op jit(solution)/shard_map/all_to_all | solution.py:118
  (129 other events, 662.1 us)
Sparse Core Ops, SparseCore 0:
  10.1 30.6 all-gather.6
  43.7 20.9 reduce-scatter.12
  67.2 21.6 reduce-scatter.14
  91.3 21.6 reduce-scatter.16
  115.3 21.6 reduce-scatter.18
  139.3 21.6 reduce-scatter.20
  163.5 21.6 reduce-scatter.22
  186.8 80.7 all-gather.10
  348.2 26.1 all-gather.8
  379.0 20.9 reduce-scatter.24
  402.5 21.6 reduce-scatter.26
  426.5 21.6 reduce-scatter.28
  450.7 21.6 reduce-scatter.30
  474.7 21.6 reduce-scatter.32
  498.8 21.6 reduce-scatter.34
  521.9 80.7 all-gather.12
where the time goes:
time: 768 us; the launch traced here: 758 us
  local copies, waits for them, and re-layouts  245 us (32%)
  matrix products  160 us (21%)
  waiting for transfers between devices  143 us (19%)
  other arithmetic  140 us (18%)
  blocking collectives  47.2 us (6%)
  between operations  17.2 us (2%)
    select_n x18, other arithmetic, mix_heads(): jnp.where(live_mask[:, position][:, None, None, None], updated, memory)  121 us
    reduce_scatter x12, waiting for transfers between devices, body(): summed = lax.psum_scatter(partials, 'dp', scatter_dimension=0, tiled=True)  85.8 us
    mul x48, local copies, waits for them, and re-layouts, mix_heads(): jnp.swapaxes(seen_part, 1, 2)[:, :, :, None]  73.4 us
    mul x48, local copies, waits for them, and re-layouts, mix_heads(): jnp.swapaxes(value_heads[:, position], 1, 2)[:, :, :, None]  71 us
    dot_general x16, matrix products, mix_heads(): jnp.einsum('bihj,bhj->bhi', memory, recept_heads[:, position], precision=...  68.7 us
    dot_general x14, matrix products, mix_heads(): jnp.einsum('bihj,bhj->bhi', memory, unit_keys[:, position], precision=hig...  57.4 us
    all_gather x2, waiting for transfers between devices, body(): gathered_in = lax.all_gather(current, 'tp', axis=0, tiled=True)  56.7 us
    dot_general x12, matrix products, body(): jnp.einsum('bsd,dc->bsc', scaled, weight[block_index], preferred_element_...  26.4 us
  transfers between devices with their start and end apart: 17, of which 6 were waited for; matrix products, arithmetic and copies ran while one was open for 68% of the time, Pallas kernels for 0%

commit v1 on v0

v1 whole, which is shorter than its diff:
```python
import functools

import jax
import jax.numpy as jnp
from jax import lax
from jax.experimental import pallas as pl
from jax.experimental.pallas import tpu as pltpu
from jax.sharding import PartitionSpec as P

HEAD = 64
BLOCKS = 2
LANES = 128
CORES = 2

group_eps = 0.00064
norm_eps = 1e-06
key_eps = 1e-06
decay_scale = 0.606531
MESH = pl.DeviceIdType.MESH
F32 = jnp.float32
BF16 = jnp.bfloat16


def remote(src, dst, send, recv, axis, peer):
    return pltpu.make_async_remote_copy(
        src_ref=src,
        dst_ref=dst,
        send_sem=send,
        recv_sem=recv,
        device_id={axis: peer},
        device_id_type=MESH,
    )


def greet(peers):
    barrier = pltpu.get_barrier_semaphore()
    for axis, peer in peers:
        pl.semaphore_signal(barrier, inc=1, device_id={axis: peer}, device_id_type=MESH)
    pl.semaphore_wait(barrier, len(peers))


def project_kernel(
    block, ntp, ndp, rows, width,
    x_ref, gain_ref, w0, w1, w2, w3, w4, w5,
    out_ref, total_ref,
    wbuf, xg, sqg, part, send_a, recv_a, send_b, recv_b, sq_a, sq_ra, sq_b, sq_rb,
    wsem, xs_sem, xr_sem, ss_sem, sr_sem, as_sem, ar_sem, bs_sem, br_sem,
    qas_sem, qar_sem, qbs_sem, qbr_sem,
):
    weights = (w0, w1, w2, w3, w4, w5)
    chunks, depth, _ = wbuf.shape
    halves = chunks // 6
    nx = ndp // CORES
    tp = lax.axis_index("tp")
    dp = lax.axis_index("dp")
    core = lax.rem(dp, CORES)
    xpos = dp // CORES
    partner = dp + 1 - 2 * core

    def load(c):
        return pltpu.make_async_copy(
            weights[c // halves].at[block, :, pl.ds((c % halves) * width, width)],
            wbuf.at[c],
            wsem.at[c],
        )

    for c in range(chunks):
        load(c).start()
    x = x_ref[...].astype(F32)
    xg[tp] = (x * gain_ref[...]).astype(BF16)
    sq = x * x
    acc = sq[:, 0:LANES]
    for k in range(1, depth // LANES):
        acc = acc + sq[:, k * LANES : (k + 1) * LANES]
    sqg[tp] = acc
    peers = [("tp", lax.rem(tp + k, ntp)) for k in range(1, ntp)]
    peers += [("dp", partner)]
    peers += [("dp", CORES * lax.rem(xpos + k, nx) + core) for k in range(1, nx)]
    greet(peers)

    gathers = []
    for k in range(1, ntp):
        peer = lax.rem(tp + k, ntp)
        cp = remote(xg.at[tp], xg.at[tp], xs_sem.at[k], xr_sem.at[k], "tp", peer)
        cq = remote(sqg.at[tp], sqg.at[tp], ss_sem.at[k], sr_sem.at[k], "tp", peer)
        cp.start()
        cq.start()
        gathers += [cp, cq]
    for k in range(1, ntp):
        src = lax.rem(tp + ntp - k, ntp)
        remote(xg.at[src], xg.at[src], xs_sem.at[k], xr_sem.at[k], "tp", src).wait_recv()
        remote(sqg.at[src], sqg.at[src], ss_sem.at[k], sr_sem.at[k], "tp", src).wait_recv()

    sq_all = sqg[...].reshape(ndp, rows, LANES)
    part_sq = [sq_all[d] for d in range(ndp)]

    def pick(parts, x_at, which):
        return jnp.where(which == 0, parts[CORES * x_at], parts[CORES * x_at + 1])

    for xd in range(nx):
        sq_a[xd] = pick(part_sq, xd, 1 - core)
        sq_b[xd] = pick(part_sq, xd, core)
    copy_qa = remote(sq_a, sq_ra, qas_sem, qar_sem, "dp", partner)
    copy_qa.start()

    def copy_a(c):
        return remote(send_a.at[c], recv_a.at[c], as_sem.at[c], ar_sem.at[c], "dp", partner)

    def copy_b(c, k):
        xd = lax.rem(xpos + k, nx)
        return remote(
            send_b.at[c, k], recv_b.at[c, k], bs_sem.at[c, k], br_sem.at[c, k],
            "dp", CORES * xd + core,
        )

    def stage_b(c):
        copy_a(c).wait_recv()
        for k in range(1, nx):
            xd = lax.rem(xpos + k, nx)
            send_b[c, k] = (part[c, CORES * xd + core] + recv_a[c, xd].astype(F32)).astype(BF16)
            copy_b(c, k).start()

    def first(c, carry):
        pltpu.make_async_copy(wbuf.at[c], wbuf.at[c], wsem.at[c]).wait()
        res = jnp.dot(
            xg[...].reshape(ndp * rows, depth), wbuf[c], preferred_element_type=F32
        )
        part[c] = res.reshape(ndp, rows, width)
        for xd in range(nx):
            send_a[c, xd] = part[c, CORES * xd + 1 - core].astype(BF16)
        copy_a(c).start()

        @pl.when(c > 0)
        def _():
            stage_b(c - 1)

        return carry

    lax.fori_loop(0, chunks, first, 0)
    copy_qa.wait_recv()
    for xd in range(nx):
        sq_b[xd] = sq_b[xd] + sq_ra[xd]
    qb = []
    for k in range(1, nx):
        xd = lax.rem(xpos + k, nx)
        cp = remote(
            sq_b.at[xd], sq_rb.at[k], qbs_sem.at[k], qbr_sem.at[k], "dp", CORES * xd + core
        )
        cp.start()
        qb.append(cp)
    stage_b(chunks - 1)

    def last(c, carry):
        own = part[c, CORES * xpos + core] + recv_a[c, xpos].astype(F32)
        for k in range(1, nx):
            copy_b(c, k).wait_recv()
            own = own + recv_b[c, k].astype(F32)
        out_ref[:, pl.ds(pl.multiple_of(c * width, width), width)] = own
        copy_a(c).wait_send()
        for k in range(1, nx):
            copy_b(c, k).wait_send()
        return carry

    lax.fori_loop(0, chunks, last, 0)
    total = sq_b[xpos]
    for k in range(1, nx):
        qb[k - 1].wait_recv()
        total = total + sq_rb[k]
    total_ref[...] = total
    copy_qa.wait_send()
    for cp in qb:
        cp.wait_send()
    for cp in gathers:
        cp.wait_send()


def project(block, ntp, ndp, rows, x, gain, weights, ident):
    here, depth = x.shape
    span = weights[0].shape[2]
    width = min(256, span)
    chunks = 6 * span // width
    nx = ndp // CORES
    dma = pltpu.SemaphoreType.DMA
    vmem = pl.BlockSpec(memory_space=pltpu.VMEM)
    hbm = pl.BlockSpec(memory_space=pl.ANY)
    return pl.pallas_call(
        functools.partial(project_kernel, block, ntp, ndp, rows, width),
        out_shape=(
            jax.ShapeDtypeStruct((rows, 6 * span), F32),
            jax.ShapeDtypeStruct((rows, LANES), F32),
        ),
        in_specs=[vmem, vmem] + [hbm] * 6,
        out_specs=(vmem, vmem),
        scratch_shapes=[
            pltpu.VMEM((chunks, depth, width), BF16),
            pltpu.VMEM((ntp, here, depth), BF16),
            pltpu.VMEM((ntp, here, LANES), F32),
            pltpu.VMEM((chunks, ndp, rows, width), F32),
            pltpu.VMEM((chunks, nx, rows, width), BF16),
            pltpu.VMEM((chunks, nx, rows, width), BF16),
            pltpu.VMEM((chunks, nx, rows, width), BF16),
            pltpu.VMEM((chunks, nx, rows, width), BF16),
            pltpu.VMEM((nx, rows, LANES), F32),
            pltpu.VMEM((nx, rows, LANES), F32),
            pltpu.VMEM((nx, rows, LANES), F32),
            pltpu.VMEM((nx, rows, LANES), F32),
            dma((chunks,)),
            dma((ntp,)), dma((ntp,)), dma((ntp,)), dma((ntp,)),
            dma((chunks,)), dma((chunks,)),
            dma((chunks, nx)), dma((chunks, nx)),
            dma, dma, dma((nx,)), dma((nx,)),
        ],
        compiler_params=pltpu.CompilerParams(
            collective_id=ident, has_side_effects=True, vmem_limit_bytes=48 * 1024 * 1024
        ),
        name="project%d" % block,
    )(x, gain, *weights)


def split_dot(a, b):
    hi = a.astype(BF16)
    lo = (a - hi.astype(F32)).astype(BF16)
    return jnp.dot(hi, b, preferred_element_type=F32) + jnp.dot(lo, b, preferred_element_type=F32)


def split_dot_right(a, b):
    hi = b.astype(BF16)
    lo = (b - hi.astype(F32)).astype(BF16)
    return jnp.dot(a, hi, preferred_element_type=F32) + jnp.dot(a, lo, preferred_element_type=F32)


def grid_of(shape, dim):
    return lax.broadcasted_iota(jnp.int32, shape, dim)


def mix_kernel(features, steps, proj_ref, total_ref, live_ref, base_ref, gain_ref, state_ref, *rest):
    gated_ref, final_ref = rest[-2], rest[-1]
    rows = proj_ref.shape[0]
    span = base_ref.shape[1]
    heads = span // HEAD
    tall = heads * steps
    inv = lax.rsqrt(jnp.sum(total_ref[...], axis=1, keepdims=True) / features + norm_eps)
    recept, keys, values, decay_pre, rate_pre, gate_pre = (
        proj_ref[:, i * span : (i + 1) * span] * inv for i in range(6)
    )
    live = live_ref[...][:, 0:1]
    seg = (grid_of((span, span), 0) // HEAD == grid_of((span, span), 1) // HEAD).astype(F32).astype(BF16)
    rb = grid_of((rows, rows), 0)
    cb = grid_of((rows, rows), 1)
    same = rb // steps == cb // steps
    lower = jnp.where(same & (cb <= rb), 1.0, 0.0).astype(BF16)
    whole = jnp.where(same, 1.0, 0.0).astype(BF16)
    unit = keys * lax.rsqrt(split_dot(keys * keys, seg) + key_eps)
    removal = unit * jax.nn.sigmoid(rate_pre) * live
    logd = -decay_scale * jax.nn.sigmoid(decay_pre + base_ref[...]) * live
    upto = split_dot_right(lower, logd)
    ends = jnp.exp(split_dot_right(whole, logd))
    back = jnp.exp(-upto)
    u_in = unit * jnp.exp(upto - logd)
    q_in = recept * jnp.exp(upto)
    r_out = removal * back
    k_out = keys * live * back
    r_end = r_out * ends
    k_end = k_out * ends
    scale_out = gain_ref[...] * jax.nn.sigmoid(gate_pre) * live

    mask = jnp.where(
        grid_of((tall, span), 0) // steps == grid_of((tall, span), 1) // HEAD, 1.0, 0.0
    )
    fold = jnp.where(
        grid_of((span, HEAD), 0) % HEAD == grid_of((span, HEAD), 1), 1.0, 0.0
    ).astype(BF16)
    tr = grid_of((tall, tall), 0)
    tc = grid_of((tall, tall), 1)
    strict_m = jnp.where(tc < tr, 1.0, 0.0)
    lower_m = jnp.where(tc <= tr, 1.0, 0.0)
    nt = (((1,), (1,)), ((), ()))
    tn = (((0,), (0,)), ((), ()))

    def exact(a, b):
        return jnp.dot(a, b, preferred_element_type=F32, precision=lax.Precision.HIGHEST)

    def quick(a, b, dims=(((1,), (0,)), ((), ()))):
        return lax.dot_general(a.astype(BF16), b.astype(BF16), dims, preferred_element_type=F32)

    for b in range(rows // steps):
        cut = slice(b * steps, (b + 1) * steps)

        def spread(a):
            return (jnp.concatenate([a[cut]] * heads, axis=0) * mask).astype(BF16)

        memory = state_ref[0, b]
        ask = jnp.concatenate([spread(u_in), spread(q_in)], axis=0)
        on_s = quick(ask, memory, nt)
        on_r = quick(ask, spread(r_out), nt)
        on_k = quick(ask, spread(k_out), nt)
        m1 = on_r[:tall] * strict_m
        m2 = on_k[:tall] * strict_m
        p_r = on_r[tall:] * lower_m
        p_k = on_k[tall:] * lower_m
        vals = jnp.dot(spread(values), fold, preferred_element_type=F32)
        seen = on_s[:tall] + quick(m2, vals)
        squared = exact(m1, m1)
        fourth = exact(squared, squared)
        seen = seen + exact(fourth, seen)
        seen = seen + exact(squared, seen)
        seen = seen - exact(m1, seen)
        read = on_s[tall:] + quick(p_k, vals) - quick(p_r, seen)
        final_ref[0, b] = (
            memory * ends[b * steps : b * steps + 1]
            + quick(vals, spread(k_end), tn)
            - quick(seen, spread(r_end), tn)
        )
        centered = read - jnp.mean(read, axis=1, keepdims=True)
        normed = centered * lax.rsqrt(
            jnp.mean(centered * centered, axis=1, keepdims=True) + group_eps
        )
        wide = jnp.concatenate([normed, normed], axis=1)
        wide = jnp.concatenate([wide] * (heads // 2), axis=1) * mask
        flat = wide[0:steps]
        for h in range(1, heads):
            flat = flat + wide[h * steps : (h + 1) * steps]
        gated_ref[cut, :] = (flat * scale_out[cut]).astype(BF16)


def mix(block, features, steps, proj, total, live, base, gain, states, earlier):
    rows = proj.shape[0]
    span = base.shape[1]
    _, held, size, _ = states.shape
    full = lambda shape: pl.BlockSpec(shape, lambda i: (0,) * len(shape))
    slab = pl.BlockSpec((1, held, size, span), lambda i: (block, 0, 0, 0))
    args = [proj, total, live, base, gain, states]
    in_specs = [full(a.shape) for a in args[:5]] + [slab]
    aliases = {}
    if earlier is not None:
        args.append(earlier)
        in_specs.append(pl.BlockSpec(memory_space=pl.ANY))
        aliases = {6: 1}
    return pl.pallas_call(
        functools.partial(mix_kernel, features, steps),
        grid=(1,),
        out_shape=(
            jax.ShapeDtypeStruct((rows, span), BF16),
            jax.ShapeDtypeStruct(states.shape, F32),
        ),
        in_specs=in_specs,
        out_specs=(full((rows, span)), slab),
        input_output_aliases=aliases,
        compiler_params=pltpu.CompilerParams(vmem_limit_bytes=48 * 1024 * 1024),
        name="mix%d" % block,
    )(*args)


def output_kernel(
    block, ntp, ndp, rows,
    gated_ref, x_ref, w_ref, out_ref,
    wbuf, gg, osend, orecv, wsem, gs_sem, gr_sem, os_sem, or_sem,
):
    here = x_ref.shape[0]
    tp = lax.axis_index("tp")
    dp = lax.axis_index("dp")
    load = pltpu.make_async_copy(w_ref.at[block], wbuf, wsem)
    load.start()
    gg[pl.ds(pl.multiple_of(dp * rows, rows), rows), :] = gated_ref[...]
    greet(
        [("dp", lax.rem(dp + k, ndp)) for k in range(1, ndp)]
        + [("tp", lax.rem(tp + k, ntp)) for k in range(1, ntp)]
    )
    sends = []
    for k in range(1, ndp):
        at = gg.at[pl.ds(pl.multiple_of(dp * rows, rows), rows), :]
        cp = remote(gated_ref, at, gs_sem.at[k], gr_sem.at[k], "dp", lax.rem(dp + k, ndp))
        cp.start()
        sends.append(cp)
    for k in range(1, ndp):
        src = lax.rem(dp + ndp - k, ndp)
        at = gg.at[pl.ds(pl.multiple_of(src * rows, rows), rows), :]
        remote(gated_ref, at, gs_sem.at[k], gr_sem.at[k], "dp", src).wait_recv()
    load.wait()

    def partial_of(peer):
        take = gg[pl.ds(pl.multiple_of(peer * here, here), here), :]
        return jnp.dot(take, wbuf[...], preferred_element_type=F32)

    def copy_o(k):
        return remote(
            osend.at[k], orecv.at[k], os_sem.at[k], or_sem.at[k], "tp", lax.rem(tp + k, ntp)
        )

    def give(k, carry):
        osend[k] = partial_of(lax.rem(tp + k, ntp)).astype(BF16)
        copy_o(k).start()
        return carry

    lax.fori_loop(1, ntp, give, 0)
    out_ref[...] = x_ref[...].astype(F32) + partial_of(tp)

    def take(k, carry):
        copy_o(k).wait_recv()
        out_ref[...] += orecv[k].astype(F32)
        copy_o(k).wait_send()
        return carry

    lax.fori_loop(1, ntp, take, 0)
    for cp in sends:
        cp.wait_send()


def output(block, ntp, ndp, gated, x, w_out, ident):
    rows, span = gated.shape
    here, depth = x.shape
    dma = pltpu.SemaphoreType.DMA
    vmem = pl.BlockSpec(memory_space=pltpu.VMEM)
    return pl.pallas_call(
        functools.partial(output_kernel, block, ntp, ndp, rows),
        out_shape=jax.ShapeDtypeStruct((here, depth), F32),
        in_specs=[vmem, vmem, pl.BlockSpec(memory_space=pl.ANY)],
        out_specs=vmem,
        scratch_shapes=[
            pltpu.VMEM((span, depth), BF16),
            pltpu.VMEM((ndp * rows, span), BF16),
            pltpu.VMEM((ntp, here, depth), BF16),
            pltpu.VMEM((ntp, here, depth), BF16),
            dma,
            dma((ndp,)), dma((ndp,)), dma((ntp,)), dma((ntp,)),
        ],
        compiler_params=pltpu.CompilerParams(
            collective_id=ident, has_side_effects=True, vmem_limit_bytes=48 * 1024 * 1024
        ),
        name="output%d" % block,
    )(gated, x, w_out)


def body(
    ntp, ndp,
    tokens, lengths, norm_gain,
    w_recept, w_key, w_value, w_decay, w_rate, w_gate,
    w_out, decay_base, out_gain, states,
):
    seqs, steps, depth = tokens.shape
    held = states.shape[1]
    rows = held * steps
    features = depth * ndp
    first_row = lax.axis_index("dp") * held
    held_lengths = lax.dynamic_slice_in_dim(lengths, first_row, held, 0)
    live = jnp.arange(steps, dtype=jnp.int32)[None, :] < held_lengths[:, None]
    live = jnp.broadcast_to(live.astype(F32).reshape(rows, 1), (rows, LANES))
    current = tokens.reshape(seqs * steps, depth)
    weights = (w_recept, w_key, w_value, w_decay, w_rate, w_gate)
    finals = None
    for block in range(BLOCKS):
        proj, total = project(
            block, ntp, ndp, rows, current, norm_gain[block : block + 1], weights, 2 * block
        )
        gated, finals = mix(
            block, features, steps, proj, total, live,
            decay_base[block : block + 1], out_gain[block : block + 1], states, finals,
        )
        current = output(block, ntp, ndp, gated, current, w_out, 2 * block + 1)
    return (current.reshape(seqs, steps, depth), finals)


def solution(mesh):
    in_specs = (
        P(("grp", "tp"), None, "dp"),
        P("grp"),
        P(None, "dp"),
        P(None, "dp", "tp"),
        P(None, "dp", "tp"),
        P(None, "dp", "tp"),
        P(None, "dp", "tp"),
        P(None, "dp", "tp"),
        P(None, "dp", "tp"),
        P(None, "tp", "dp"),
        P(None, "tp"),
        P(None, "tp"),
        P(None, ("grp", "dp"), None, "tp"),
    )
    out_specs = (P(("grp", "tp"), None, "dp"), P(None, ("grp", "dp"), None, "tp"))
    run = functools.partial(body, mesh.shape["tp"], mesh.shape["dp"])
    return jax.shard_map(run, mesh=mesh, in_specs=in_specs, out_specs=out_specs, check_vma=False)
```

time: 768 us -> 131 us (0.17); the launches traced: 758 us -> 131 us
  local copies, waits for them, and re-layouts: 245 us -> 7.26 us
  matrix products: 160 us -> 0 us
  waiting for transfers between devices: 143 us -> 0 us
  other arithmetic: 140 us -> 0.07 us
  Pallas kernels: 0 us -> 123 us
  blocking collectives: 47.2 us -> 0 us
  between operations: 17.2 us -> 0.72 us
    dot_general x44 -> x0, matrix products: 160 us -> none  [the longest x16 68.7 us: mix_heads(): jnp.einsum('bihj,bhj->bhi', memory, recept_heads[:, position], precision=...]
    mul x116 -> x0, local copies, waits for them, and re-layouts: 152 us -> none  [the longest x48 73.4 us: mix_heads(): jnp.swapaxes(seen_part, 1, 2)[:, :, :, None]]
    pallas_call x0 -> x6, Pallas kernels: none -> 123 us  [the longest x2 61.8 us: project(): pl.pallas_call(functools.partial(project_kernel, block, ntp, ndp, rows, w...]
    select_n x18 -> x0, other arithmetic: 121 us -> none  [mix_heads(): jnp.where(live_mask[:, position][:, None, None, None], updated, memory)]
    reduce_scatter x12 -> x0, waiting for transfers between devices: 85.8 us -> none  [body(): summed = lax.psum_scatter(partials, 'dp', scatter_dimension=0, tiled=True)]
    all_gather x4 -> x0, waiting for transfers between devices: 56.7 us -> none  [the longest x2 56.7 us: body(): gathered_in = lax.all_gather(current, 'tp', axis=0, tiled=True)]
    unnamed x2 -> x0, blocking collectives: 21.4 us -> none
    unnamed x367 -> x15, local copies, waits for them, and re-layouts: 26.2 us -> 4.82 us
  transfers between devices with their start and end apart: 17 -> 0, of which waited for: 6 -> 0; matrix products, arithmetic and copies ran while one was open for 68% -> 0% of each run, Pallas kernels for 0% -> 0%
where the time goes in v1:
time: 131 us
  Pallas kernels  123 us (94%)
  local copies, waits for them, and re-layouts  7.26 us (6%)
    pallas_call x2, Pallas kernels, project(): pl.pallas_call(functools.partial(project_kernel, block, ntp, ndp, rows, w...  61.8 us
    pallas_call x2, Pallas kernels, output(): pl.pallas_call(functools.partial(output_kernel, block, ntp, ndp, rows), o...  39.8 us
    pallas_call x2, Pallas kernels, mix(): pl.pallas_call(functools.partial(mix_kernel, features, steps), grid=(1,),...  21 us
    unnamed x15, local copies, waits for them, and re-layouts  4.82 us

profile of v1, /device:TPU:0, one launch (start us, length us, event | category | flops | bytes accessed | tf_op | source)
XLA Modules:
  0.0 130.8 jit_solution(3615094109559551676)
XLA Ops:
  0.6 0.7 dynamic_slice.3
  1.4 0.1 fusion
  1.4 0.1 reshape.31
  1.5 0.8 fusion.2
  2.3 0.8 fusion.1
  3.1 0.1 broadcast_in_dim.2.live_ref
  3.2 0.0 copy-start.2
  3.2 1.6 %copy-done.2 = bf16[2,1024,512]{2,1,0:T(8,128)(2,1)S(1)} copy-done((bf16[2,1024,512]{2,1,0:T(8,128)(2,1)S(1)}, bf16[2,1024,512]{2,1,0:T(8,128)(2,1)}, u32[]{:S(2)}) %copy-start.2) | copy-done | bytes 2097176
  4.8 0.0 copy-start.4
  4.8 1.6 %copy-done.4 = bf16[2,1024,512]{2,1,0:T(8,128)(2,1)S(1)} copy-done((bf16[2,1024,512]{2,1,0:T(8,128)(2,1)S(1)}, bf16[2,1024,512]{2,1,0:T(8,128)(2,1)}, u32[]{:S(2)}) %copy-start.4) | copy-done | bytes 2097176
  6.3 0.0 copy-start.6
  6.4 0.9 copy-done.6
  7.3 0.0 copy-start
  7.3 0.0 copy-start.5
  7.3 31.1 %project0.1 = (f32[64,3072]{1,0:T(8,128)S(1)}, f32[64,128]{1,0:T(8,128)S(1)}) custom-call(bf16[64,1024]{1,0:T(8,128)(2,1)S(1)} %bitcast.3, f32[1,1024]{1,0:T(1,128)S(1)} %get-tuple-element.19.gain_ref, bf16[2,1024,512]{2,1,0:T(8,128)(2,1)S(1)} %copy-done.2, bf16[2,1024,512]{2,1,0:T(8,128)(2,1)S(1)} %copy-done.4, bf16[2,1024,512]{2,1,0:T(8,128)(2,1)} %w2.3, ...), custom_call_target="tpu_custom_call" | custom-call | tf_op jit(solution)/shard_map/project0/pallas_call | solution.py:186
  38.4 0.0 copy-start.1
  38.4 0.0 copy-done
  38.4 0.0 copy-start.3
  38.4 10.5 %mix0.1 = (bf16[64,512]{1,0:T(8,128)(2,1)S(1)}, f32[2,8,64,512]{3,2,1,0:T(8,128)}) custom-call(f32[64,3072]{1,0:T(8,128)S(1)} %get-tuple-element.10.proj_ref, f32[64,128]{1,0:T(8,128)S(1)} %get-tuple-element.11.total_ref, f32[64,128]{1,0:T(8,128)S(1)} %broadcast_in_dim.2.live_ref, f32[1,512]{1,0:T(1,128)S(1)} %get-tuple-element.24.base_ref, ...), custom_call_target="tpu_custom_call" | custom-call | tf_op jit(solution)/shard_map/mix0/pallas_call | solution.py:339
  48.9 0.0 copy-done.1
  48.9 19.9 %output0.1.x_ref = f32[64,1024]{1,0:T(8,128)S(1)} custom-call(bf16[64,512]{1,0:T(8,128)(2,1)S(1)} %get-tuple-element.12.gated_ref, bf16[64,1024]{1,0:T(8,128)(2,1)S(1)} %bitcast.4, bf16[2,512,1024]{2,1,0:T(8,128)(2,1)S(1)} %copy-done.1), custom_call_target="tpu_custom_call" | custom-call | tf_op jit(solution)/shard_map/output0/pallas_call | solution.py:414
  68.8 0.0 copy-done.5
  68.8 0.0 copy-done.3
  68.8 30.7 %project1.1 = (f32[64,3072]{1,0:T(8,128)S(1)}, f32[64,128]{1,0:T(8,128)S(1)}) custom-call(f32[64,1024]{1,0:T(8,128)S(1)} %output0.1.x_ref, f32[1,1024]{1,0:T(1,128)S(1)} %get-tuple-element.18.gain_ref, bf16[2,1024,512]{2,1,0:T(8,128)(2,1)S(1)} %copy-done.3, bf16[2,1024,512]{2,1,0:T(8,128)(2,1)S(1)} %copy-done.5, bf16[2,1024,512]{2,1,0:T(8,128)(2,1)} %w2.3, ...), custom_call_target="tpu_custom_call" | custom-call | tf_op jit(solution)/shard_map/project1/pallas_call | solution.py:186
  99.6 10.5 %mix1.1 = (bf16[64,512]{1,0:T(8,128)(2,1)S(1)}, f32[2,8,64,512]{3,2,1,0:T(8,128)}) custom-call(f32[64,3072]{1,0:T(8,128)S(1)} %get-tuple-element.13.proj_ref, f32[64,128]{1,0:T(8,128)S(1)} %get-tuple-element.14.total_ref, f32[64,128]{1,0:T(8,128)S(1)} %broadcast_in_dim.2.live_ref, ...), custom_call_target="tpu_custom_call", output_to_operand_aliasing={{1}: (6, {})} | custom-call | tf_op jit(solution)/shard_map/mix1/pallas_call | solution.py:339
  110.1 20.0 %output1.1 = f32[64,1024]{1,0:T(8,128)S(1)} custom-call(bf16[64,512]{1,0:T(8,128)(2,1)S(1)} %get-tuple-element.16.gated_ref, f32[64,1024]{1,0:T(8,128)S(1)} %output0.1.x_ref, bf16[2,512,1024]{2,1,0:T(8,128)(2,1)S(1)} %copy-done.1), custom_call_target="tpu_custom_call" | custom-call | tf_op jit(solution)/shard_map/output1/pallas_call | solution.py:414
  130.1 0.7 copy.18
Async XLA Ops:
  3.2 1.6 %copy-start.2 = (bf16[2,1024,512]{2,1,0:T(8,128)(2,1)S(1)}, bf16[2,1024,512]{2,1,0:T(8,128)(2,1)}, u32[]{:S(2)}) copy-start(bf16[2,1024,512]{2,1,0:T(8,128)(2,1)} %w0.3) | copy-start | bytes 6291460
  4.8 1.6 %copy-start.4 = (bf16[2,1024,512]{2,1,0:T(8,128)(2,1)S(1)}, bf16[2,1024,512]{2,1,0:T(8,128)(2,1)}, u32[]{:S(2)}) copy-start(bf16[2,1024,512]{2,1,0:T(8,128)(2,1)} %w1.3) | copy-start | bytes 6291460
  6.3 0.9 copy-start.6
  7.3 31.1 %copy-start = (f32[2,8,64,512]{3,2,1,0:T(8,128)S(1)}, f32[2,8,64,512]{3,2,1,0:T(8,128)}, u32[]{:S(2)}) copy-start(f32[2,8,64,512]{3,2,1,0:T(8,128)} %state_ref.3) | copy-start | bytes 6291460
  7.3 61.6 %copy-start.5 = (bf16[2,1024,512]{2,1,0:T(8,128)(2,1)S(1)}, bf16[2,1024,512]{2,1,0:T(8,128)(2,1)}, u32[]{:S(2)}) copy-start(bf16[2,1024,512]{2,1,0:T(8,128)(2,1)} %w1.3) | copy-start | bytes 6291460
  38.4 10.6 %copy-start.1 = (bf16[2,512,1024]{2,1,0:T(8,128)(2,1)S(1)}, bf16[2,512,1024]{2,1,0:T(8,128)(2,1)}, u32[]{:S(2)}) copy-start(bf16[2,512,1024]{2,1,0:T(8,128)(2,1)} %w_ref.3) | copy-start | bytes 6291460
  38.4 30.4 %copy-start.3 = (bf16[2,1024,512]{2,1,0:T(8,128)(2,1)S(1)}, bf16[2,1024,512]{2,1,0:T(8,128)(2,1)}, u32[]{:S(2)}) copy-start(bf16[2,1024,512]{2,1,0:T(8,128)(2,1)} %w0.3) | copy-start | bytes 6291460

commit v2 on v1

--- a/solution.py
+++ b/solution.py
@@ -43,7 +43,7 @@
     block, ntp, ndp, rows, width,
     x_ref, gain_ref, w0, w1, w2, w3, w4, w5,
     out_ref, total_ref,
-    wbuf, xg, sqg, part, send_a, recv_a, send_b, recv_b, sq_a, sq_ra, sq_b, sq_rb,
+    wbuf, xg, sqg, part, recv_a, send_b, recv_b, sq_a, sq_ra, sq_b, sq_rb,
     wsem, xs_sem, xr_sem, ss_sem, sr_sem, as_sem, ar_sem, bs_sem, br_sem,
     qas_sem, qar_sem, qbs_sem, qbr_sem,
 ):
@@ -67,7 +67,7 @@
     for c in range(chunks):
         load(c).start()
     x = x_ref[...].astype(F32)
-    xg[tp] = (x * gain_ref[...]).astype(BF16)
+    xg[tp] = (x * gain_ref[block : block + 1, :]).astype(BF16)
     sq = x * x
     acc = sq[:, 0:LANES]
     for k in range(1, depth // LANES):
@@ -104,7 +104,7 @@
     copy_qa.start()
 
     def copy_a(c):
-        return remote(send_a.at[c], recv_a.at[c], as_sem.at[c], ar_sem.at[c], "dp", partner)
+        return remote(part.at[c, 1 - core], recv_a.at[c], as_sem.at[c], ar_sem.at[c], "dp", partner)
 
     def copy_b(c, k):
         xd = lax.rem(xpos + k, nx)
@@ -117,7 +117,7 @@
         copy_a(c).wait_recv()
         for k in range(1, nx):
             xd = lax.rem(xpos + k, nx)
-            send_b[c, k] = (part[c, CORES * xd + core] + recv_a[c, xd].astype(F32)).astype(BF16)
+            send_b[c, k] = (part[c, core, xd] + recv_a[c, xd]).astype(BF16)
             copy_b(c, k).start()
 
     def first(c, carry):
@@ -125,9 +125,8 @@
         res = jnp.dot(
             xg[...].reshape(ndp * rows, depth), wbuf[c], preferred_element_type=F32
         )
-        part[c] = res.reshape(ndp, rows, width)
-        for xd in range(nx):
-            send_a[c, xd] = part[c, CORES * xd + 1 - core].astype(BF16)
+        for d in range(ndp):
+            part[c, d % CORES, d // CORES] = res[d * rows : (d + 1) * rows]
         copy_a(c).start()
 
         @pl.when(c > 0)
@@ -151,7 +150,7 @@
     stage_b(chunks - 1)
 
     def last(c, carry):
-        own = part[c, CORES * xpos + core] + recv_a[c, xpos].astype(F32)
+        own = part[c, core, xpos] + recv_a[c, xpos]
         for k in range(1, nx):
             copy_b(c, k).wait_recv()
             own = own + recv_b[c, k].astype(F32)
@@ -182,7 +181,7 @@
     nx = ndp // CORES
     dma = pltpu.SemaphoreType.DMA
     vmem = pl.BlockSpec(memory_space=pltpu.VMEM)
-    hbm = pl.BlockSpec(memory_space=pl.ANY)
+    hbm = pl.BlockSpec(memory_space=pltpu.HBM)
     return pl.pallas_call(
         functools.partial(project_kernel, block, ntp, ndp, rows, width),
         out_shape=(
@@ -195,9 +194,8 @@
             pltpu.VMEM((chunks, depth, width), BF16),
             pltpu.VMEM((ntp, here, depth), BF16),
             pltpu.VMEM((ntp, here, LANES), F32),
-            pltpu.VMEM((chunks, ndp, rows, width), F32),
-            pltpu.VMEM((chunks, nx, rows, width), BF16),
-            pltpu.VMEM((chunks, nx, rows, width), BF16),
+            pltpu.VMEM((chunks, CORES, nx, rows, width), F32),
+            pltpu.VMEM((chunks, nx, rows, width), F32),
             pltpu.VMEM((chunks, nx, rows, width), BF16),
             pltpu.VMEM((chunks, nx, rows, width), BF16),
             pltpu.VMEM((nx, rows, LANES), F32),
@@ -211,21 +209,24 @@
             dma, dma, dma((nx,)), dma((nx,)),
         ],
         compiler_params=pltpu.CompilerParams(
-            collective_id=ident, has_side_effects=True, vmem_limit_bytes=48 * 1024 * 1024
+            collective_id=ident, has_side_effects=True, vmem_limit_bytes=65500000
         ),
         name="project%d" % block,
     )(x, gain, *weights)
 
 
+def halves(a):
+    hi = a.astype(BF16)
+    return hi, (a - hi.astype(F32)).astype(BF16)
+
+
 def split_dot(a, b):
-    hi = a.astype(BF16)
-    lo = (a - hi.astype(F32)).astype(BF16)
+    hi, lo = halves(a)
     return jnp.dot(hi, b, preferred_element_type=F32) + jnp.dot(lo, b, preferred_element_type=F32)
 
 
 def split_dot_right(a, b):
-    hi = b.astype(BF16)
-    lo = (b - hi.astype(F32)).astype(BF16)
+    hi, lo = halves(b)
     return jnp.dot(a, hi, preferred_element_type=F32) + jnp.dot(a, lo, preferred_element_type=F32)
 
 
@@ -233,7 +234,7 @@
     return lax.broadcasted_iota(jnp.int32, shape, dim)
 
 
-def mix_kernel(features, steps, proj_ref, total_ref, live_ref, base_ref, gain_ref, state_ref, *rest):
+def mix_kernel(block, features, steps, proj_ref, total_ref, live_ref, base_ref, gain_ref, state_ref, *rest):
     gated_ref, final_ref = rest[-2], rest[-1]
     rows = proj_ref.shape[0]
     span = base_ref.shape[1]
@@ -252,7 +253,7 @@
     whole = jnp.where(same, 1.0, 0.0).astype(BF16)
     unit = keys * lax.rsqrt(split_dot(keys * keys, seg) + key_eps)
     removal = unit * jax.nn.sigmoid(rate_pre) * live
-    logd = -decay_scale * jax.nn.sigmoid(decay_pre + base_ref[...]) * live
+    logd = -decay_scale * jax.nn.sigmoid(decay_pre + base_ref[block : block + 1, :]) * live
     upto = split_dot_right(lower, logd)
     ends = jnp.exp(split_dot_right(whole, logd))
     back = jnp.exp(-upto)
@@ -262,7 +263,7 @@
     k_out = keys * live * back
     r_end = r_out * ends
     k_end = k_out * ends
-    scale_out = gain_ref[...] * jax.nn.sigmoid(gate_pre) * live
+    scale_out = gain_ref[block : block + 1, :] * jax.nn.sigmoid(gate_pre) * live
 
     mask = jnp.where(
         grid_of((tall, span), 0) // steps == grid_of((tall, span), 1) // HEAD, 1.0, 0.0
@@ -287,30 +288,37 @@
         cut = slice(b * steps, (b + 1) * steps)
 
         def spread(a):
-            return (jnp.concatenate([a[cut]] * heads, axis=0) * mask).astype(BF16)
+            return jnp.concatenate([a[cut]] * heads, axis=0) * mask
 
         memory = state_ref[0, b]
-        ask = jnp.concatenate([spread(u_in), spread(q_in)], axis=0)
-        on_s = quick(ask, memory, nt)
-        on_r = quick(ask, spread(r_out), nt)
-        on_k = quick(ask, spread(k_out), nt)
+        m_hi, m_lo = halves(memory)
+        a_hi, a_lo = halves(jnp.concatenate([spread(u_in), spread(q_in)], axis=0))
+        k_hi, k_lo = halves(spread(k_out))
+        v_all = jnp.concatenate(halves(spread(values)), axis=0)
+        both = quick(a_hi, jnp.concatenate([m_hi, m_lo, k_hi, k_lo], axis=0), nt)
+        tail = quick(a_lo, jnp.concatenate([m_hi, k_hi], axis=0), nt)
+        on_r = quick(a_hi, spread(r_out), nt)
+        at = 2 * HEAD
+        on_s = both[:, :HEAD] + both[:, HEAD:at] + tail[:, :HEAD]
+        on_k = both[:, at : at + tall] + both[:, at + tall :] + tail[:, HEAD:]
         m1 = on_r[:tall] * strict_m
         m2 = on_k[:tall] * strict_m
         p_r = on_r[tall:] * lower_m
         p_k = on_k[tall:] * lower_m
-        vals = jnp.dot(spread(values), fold, preferred_element_type=F32)
+        folded = quick(v_all, fold)
+        vals = folded[:tall] + folded[tall:]
         seen = on_s[:tall] + quick(m2, vals)
         squared = exact(m1, m1)
         fourth = exact(squared, squared)
         seen = seen + exact(fourth, seen)
         seen = seen + exact(squared, seen)
         seen = seen - exact(m1, seen)
-        read = on_s[tall:] + quick(p_k, vals) - quick(p_r, seen)
-        final_ref[0, b] = (
-            memory * ends[b * steps : b * steps + 1]
-            + quick(vals, spread(k_end), tn)
-            - quick(seen, spread(r_end), tn)
-        )
+        read = on_s[tall:] + exact(p_k, vals) - quick(p_r, seen)
+        v_hi, v_lo = halves(vals)
+        e_hi, e_lo = halves(spread(k_end))
+        left = jnp.concatenate([v_hi, v_lo, v_hi, (-seen).astype(BF16)], axis=0)
+        right = jnp.concatenate([e_hi, e_hi, e_lo, spread(r_end).astype(BF16)], axis=0)
+        final_ref[0, b] = memory * ends[b * steps : b * steps + 1] + quick(left, right, tn)
         centered = read - jnp.mean(read, axis=1, keepdims=True)
         normed = centered * lax.rsqrt(
             jnp.mean(centered * centered, axis=1, keepdims=True) + group_eps
@@ -337,7 +345,7 @@
         in_specs.append(pl.BlockSpec(memory_space=pl.ANY))
         aliases = {6: 1}
     return pl.pallas_call(
-        functools.partial(mix_kernel, features, steps),
+        functools.partial(mix_kernel, block, features, steps),
         grid=(1,),
         out_shape=(
             jax.ShapeDtypeStruct((rows, span), BF16),
@@ -414,7 +422,7 @@
     return pl.pallas_call(
         functools.partial(output_kernel, block, ntp, ndp, rows),
         out_shape=jax.ShapeDtypeStruct((here, depth), F32),
-        in_specs=[vmem, vmem, pl.BlockSpec(memory_space=pl.ANY)],
+        in_specs=[vmem, vmem, pl.BlockSpec(memory_space=pltpu.HBM)],
         out_specs=vmem,
         scratch_shapes=[
             pltpu.VMEM((span, depth), BF16),
@@ -450,11 +458,11 @@
     finals = None
     for block in range(BLOCKS):
         proj, total = project(
-            block, ntp, ndp, rows, current, norm_gain[block : block + 1], weights, 2 * block
+            block, ntp, ndp, rows, current, norm_gain, weights, 2 * block
         )
         gated, finals = mix(
             block, features, steps, proj, total, live,
-            decay_base[block : block + 1], out_gain[block : block + 1], states, finals,
+            decay_base, out_gain, states, finals,
         )
         current = output(block, ntp, ndp, gated, current, w_out, 2 * block + 1)
     return (current.reshape(seqs, steps, depth), finals)

time: 131 us -> 139 us (1.061)
  Pallas kernels: 123 us -> 128 us
  local copies, waits for them, and re-layouts: 7.26 us -> 9.27 us
    pallas_call x2, Pallas kernels: 61.8 us -> 65.6 us  [project(): pl.pallas_call(functools.partial(project_kernel, block, ntp, ndp, rows, w...]
    unnamed x15 -> x27, local copies, waits for them, and re-layouts: 4.82 us -> 8.38 us
    pallas_call x2, Pallas kernels: 21 us -> 23 us  [mix(): pl.pallas_call(functools.partial(mix_kernel, block, features, steps), gri...]
    slice x2 -> x0, local copies, waits for them, and re-layouts: 1.56 us -> none  [the longest x1 0.78 us: body(): norm_gain[block:block + 1]]
where the time goes in v2:
time: 139 us; the launch traced here: 138 us
  Pallas kernels  128 us (92%)
  local copies, waits for them, and re-layouts  9.27 us (7%)
    pallas_call x2, Pallas kernels, project(): pl.pallas_call(functools.partial(project_kernel, block, ntp, ndp, rows, w...  65.6 us
    pallas_call x2, Pallas kernels, output(): pl.pallas_call(functools.partial(output_kernel, block, ntp, ndp, rows), o...  39.4 us
    pallas_call x2, Pallas kernels, mix(): pl.pallas_call(functools.partial(mix_kernel, block, features, steps), gri...  23 us
    unnamed x27, local copies, waits for them, and re-layouts  8.38 us

profile of v2, /device:TPU:0, one launch (start us, length us, event | category | flops | bytes accessed | tf_op | source)
XLA Modules:
  0.0 138.1 jit_solution(17495870819752128064)
XLA Ops:
  0.6 0.7 dynamic_slice.3
  1.4 0.1 fusion
  1.4 0.1 reshape.31
  1.5 0.1 broadcast_in_dim.2.live_ref
  1.6 0.0 copy-start.11
  1.6 0.0 copy-start.12
  1.6 0.0 copy-start.8
  1.6 32.9 %project0.1 = (f32[64,3072]{1,0:T(8,128)}, f32[64,128]{1,0:T(8,128)}) custom-call(bf16[64,1024]{1,0:T(8,128)(2,1)} %bitcast.3, f32[2,1024]{1,0:T(2,128)} %gain_ref.6, bf16[2,1024,512]{2,1,0:T(8,128)(2,1)} %w0.3, bf16[2,1024,512]{2,1,0:T(8,128)(2,1)} %w1.3, bf16[2,1024,512]{2,1,0:T(8,128)(2,1)} %w2.3, bf16[2,1024,512]{2,1,0:T(8,128)(2,1)} %w3.3, ...), custom_call_target="tpu_custom_call" | custom-call | tf_op jit(solution)/shard_map/project0/pallas_call | solution.py:185
  34.5 0.0 copy-done.11
  34.6 0.0 copy-done.12
  34.6 0.0 copy-start
  34.6 1.6 %copy-done = f32[2,8,64,512]{3,2,1,0:T(8,128)S(1)} copy-done((f32[2,8,64,512]{3,2,1,0:T(8,128)S(1)}, f32[2,8,64,512]{3,2,1,0:T(8,128)}, u32[]{:S(2)}) %copy-start) | copy-done | bytes 2097176
  36.2 0.0 copy-start.7
  36.2 1.1 copy-done.7
  37.3 0.0 copy-start.10
  37.3 0.8 copy-done.10
  38.1 0.0 copy-start.2
  38.1 11.5 %mix0.1 = (bf16[64,512]{1,0:T(8,128)(2,1)S(1)}, f32[2,8,64,512]{3,2,1,0:T(8,128)}) custom-call(f32[64,3072]{1,0:T(8,128)S(1)} %copy-done.7, f32[64,128]{1,0:T(8,128)S(1)} %copy-done.10, f32[64,128]{1,0:T(8,128)S(1)} %broadcast_in_dim.2.live_ref, f32[2,512]{1,0:T(2,128)S(1)} %copy-done.11, f32[2,512]{1,0:T(2,128)S(1)} %copy-done.12, f32[2,8,64,512]{3,2,1,0:T(8,128)S(1)} %copy-done), custom_call_target="tpu_custom_call" | custom-call | tf_op jit(solution)/shard_map/mix0/pallas_call | solution.py:347
  49.6 0.0 copy-done.8
  49.6 0.0 copy-done.2
  49.6 19.6 %output0.1.x_ref = f32[64,1024]{1,0:T(8,128)S(1)} custom-call(bf16[64,512]{1,0:T(8,128)(2,1)S(1)} %get-tuple-element.12.gated_ref, bf16[64,1024]{1,0:T(8,128)(2,1)S(1)} %bitcast.4, bf16[2,512,1024]{2,1,0:T(8,128)(2,1)S(1)} %copy-done.2), custom_call_target="tpu_custom_call" | custom-call | tf_op jit(solution)/shard_map/output0/pallas_call | solution.py:422
  69.2 0.0 copy-start.4
  69.2 0.7 copy-done.4
  69.9 32.7 %project1.1 = (f32[64,3072]{1,0:T(8,128)}, f32[64,128]{1,0:T(8,128)}) custom-call(f32[64,1024]{1,0:T(8,128)} %copy-done.4, f32[2,1024]{1,0:T(2,128)} %gain_ref.6, bf16[2,1024,512]{2,1,0:T(8,128)(2,1)} %w0.3, bf16[2,1024,512]{2,1,0:T(8,128)(2,1)} %w1.3, bf16[2,1024,512]{2,1,0:T(8,128)(2,1)} %w2.3, bf16[2,1024,512]{2,1,0:T(8,128)(2,1)} %w3.3, ...), custom_call_target="tpu_custom_call" | custom-call | tf_op jit(solution)/shard_map/project1/pallas_call | solution.py:185
  102.6 0.0 copy-start.1
  102.6 1.6 %copy-done.1 = f32[2,8,64,512]{3,2,1,0:T(8,128)S(1)} copy-done((f32[2,8,64,512]{3,2,1,0:T(8,128)S(1)}, f32[2,8,64,512]{3,2,1,0:T(8,128)}, u32[]{:S(2)}) %copy-start.1) | copy-done | bytes 2097176
  104.2 0.0 copy-start.6
  104.2 1.1 copy-done.6
  105.3 0.0 copy-start.9
  105.3 0.8 copy-done.9
  106.1 0.0 copy-start.3
  106.1 0.0 copy-start.5
  106.1 11.5 %mix1.1 = (bf16[64,512]{1,0:T(8,128)(2,1)S(1)}, f32[2,8,64,512]{3,2,1,0:T(8,128)}) custom-call(f32[64,3072]{1,0:T(8,128)S(1)} %copy-done.6, f32[64,128]{1,0:T(8,128)S(1)} %copy-done.9, f32[64,128]{1,0:T(8,128)S(1)} %broadcast_in_dim.2.live_ref, f32[2,512]{1,0:T(2,128)S(1)} %copy-done.11, f32[2,512]{1,0:T(2,128)S(1)} %copy-done.12, ...), custom_call_target="tpu_custom_call", output_to_operand_aliasing={{1}: (6, {})} | custom-call | tf_op jit(solution)/shard_map/mix1/pallas_call | solution.py:347
  117.6 0.0 copy-done.3
  117.6 0.0 copy-done.5
  117.6 19.8 %output1.1 = f32[64,1024]{1,0:T(8,128)S(1)} custom-call(bf16[64,512]{1,0:T(8,128)(2,1)S(1)} %get-tuple-element.16.gated_ref, f32[64,1024]{1,0:T(8,128)S(1)} %copy-done.5, bf16[2,512,1024]{2,1,0:T(8,128)(2,1)S(1)} %copy-done.3), custom_call_target="tpu_custom_call" | custom-call | tf_op jit(solution)/shard_map/output1/pallas_call | solution.py:422
  137.3 0.7 copy.18
Async XLA Ops:
  1.6 33.0 %copy-start.11 = (f32[2,512]{1,0:T(2,128)S(1)}, f32[2,512]{1,0:T(2,128)}, u32[]{:S(2)}) copy-start(f32[2,512]{1,0:T(2,128)} %base_ref.3) | copy-start | bytes 12292
  1.6 33.0 %copy-start.12 = (f32[2,512]{1,0:T(2,128)S(1)}, f32[2,512]{1,0:T(2,128)}, u32[]{:S(2)}) copy-start(f32[2,512]{1,0:T(2,128)} %gain_ref.7) | copy-start | bytes 12292
  1.6 48.0 %copy-start.8 = (bf16[8,8,1024]{2,1,0:T(8,128)(2,1)S(1)}, bf16[8,8,1024]{2,1,0:T(8,128)(2,1)}, u32[]{:S(2)}) copy-start(bf16[8,8,1024]{2,1,0:T(8,128)(2,1)} %param.13) | copy-start | bytes 393220
  34.6 1.6 %copy-start = (f32[2,8,64,512]{3,2,1,0:T(8,128)S(1)}, f32[2,8,64,512]{3,2,1,0:T(8,128)}, u32[]{:S(2)}) copy-start(f32[2,8,64,512]{3,2,1,0:T(8,128)} %state_ref.3) | copy-start | bytes 6291460
  36.2 1.1 copy-start.7
  37.3 0.8 copy-start.10
  38.1 11.5 %copy-start.2 = (bf16[2,512,1024]{2,1,0:T(8,128)(2,1)S(1)}, bf16[2,512,1024]{2,1,0:T(8,128)(2,1)}, u32[]{:S(2)}) copy-start(bf16[2,512,1024]{2,1,0:T(8,128)(2,1)} %w_ref.3) | copy-start | bytes 6291460
  69.2 0.7 copy-start.4
  102.6 1.6 %copy-start.1 = (f32[2,8,64,512]{3,2,1,0:T(8,128)S(1)}, f32[2,8,64,512]{3,2,1,0:T(8,128)}, u32[]{:S(2)}) copy-start(f32[2,8,64,512]{3,2,1,0:T(8,128)} %state_ref.3) | copy-start | bytes 6291460
  104.2 1.1 copy-start.6
  105.3 0.8 copy-start.9
  106.1 11.5 %copy-start.3 = (bf16[2,512,1024]{2,1,0:T(8,128)(2,1)S(1)}, bf16[2,512,1024]{2,1,0:T(8,128)(2,1)}, u32[]{:S(2)}) copy-start(bf16[2,512,1024]{2,1,0:T(8,128)(2,1)} %w_ref.3) | copy-start | bytes 6291460
  106.1 11.5 %copy-start.5 = (f32[64,1024]{1,0:T(8,128)S(1)}, f32[64,1024]{1,0:T(8,128)}, u32[]{:S(2)}) copy-start(f32[64,1024]{1,0:T(8,128)} %copy-done.4) | copy-start | bytes 786436
